TPU v7x, 256 devices: a whole 4x4x8 slice. The times are simulated.
256 devices in a mesh: kv: 32 (over z, y), tp: 8 (over x, core).
Axes of the slice: x: 4, y: 4, z: 8, core: 2. Of those that a mesh axis runs over, the one named last changes fastest.
Arguments:
- residual_in: bfloat16 [256, 2048], P(None, ('kv', 'tp')), may hold values from -14 to 14
- delta_state: float32 [256, 32, 128, 128], P('kv', 'tp'), may hold values from -1 to 1
- norm_gain_first: float32 [2048], P('kv'), may hold values from 0.1 to 1.9
- gate_first: bfloat16 [2048, 5632], P('kv', 'tp'), may hold values from -0.125 to 0.125
- up_first: bfloat16 [2048, 5632], P('kv', 'tp'), may hold values from -0.125 to 0.125
- down_first: bfloat16 [5632, 2048], P('tp', 'kv'), may hold values from -0.15625 to 0.15625
- norm_gain_mixer: float32 [2048], P('kv'), may hold values from 0.1 to 1.9
- query_weight: bfloat16 [2048, 2048], P('kv', 'tp'), may hold values from -0.125 to 0.125
- key_weight: bfloat16 [2048, 2048], P('kv', 'tp'), may hold values from -0.125 to 0.125
- value_weight: bfloat16 [2048, 4096], P('kv', 'tp'), may hold values from -0.125 to 0.125
- output_gate_weight: bfloat16 [2048, 4096], P('kv', 'tp'), may hold values from -0.125 to 0.125
- beta_weight: bfloat16 [2048, 32], P('kv'), may hold values from -0.125 to 0.125
- decay_weight: bfloat16 [2048, 32], P('kv'), may hold values from -0.125 to 0.125
- decay_rate: float32 [32], P('tp'), may hold values from -2.3 to 1.1
- decay_bias: float32 [32], P('tp'), may hold values from -1 to 1
- head_gain: float32 [128], replicated, may hold values from 0.1 to 1.9
- out_weight: bfloat16 [4096, 2048], P('tp', 'kv'), may hold values from -0.125 to 0.125
- norm_gain_second: float32 [2048], P('kv'), may hold values from 0.1 to 1.9
- gate_second: bfloat16 [2048, 5632], P('kv', 'tp'), may hold values from -0.125 to 0.125
- up_second: bfloat16 [2048, 5632], P('kv', 'tp'), may hold values from -0.125 to 0.125
- down_second: bfloat16 [5632, 2048], P('tp', 'kv'), may hold values from -0.15625 to 0.15625
Outputs:
- residual_out: bfloat16 [256, 2048], P(None, ('kv', 'tp'))
- delta_state_out: float32 [256, 32, 128, 128], P('kv', 'tp')
All inputs are finite; a program needn't handle non-finite values.
Results may differ from a plain program's by a relative error of at most 0.03.
Values may be sent and summed in bfloat16 or wider, within the bound.
A program may use at most 64 MiB of HBM per device.

v0:
```python
import jax
import jax.numpy as jnp
from jax import lax
from jax.sharding import PartitionSpec as P

D = 2048
epsilon = 1e-06


def in_blocks(value, dim, size):
    before, after = (value.shape[:dim], value.shape[dim + 1 :])
    return jnp.moveaxis(value.reshape(*before, size, -1, *after), dim, 0)


def summed_on_arrival(value, axis, dim):
    blocks = in_blocks(value, dim, lax.axis_size(axis))
    arrived = lax.all_to_all(blocks, axis, split_axis=0, concat_axis=0, tiled=True)
    return arrived.astype(jnp.float32).sum(axis=0)


def side_by_side(arrays, axis, dim, along):
    columns = [a.reshape(*a.shape[:along], -1) for a in arrays]
    both = jnp.concatenate(columns, axis=along)
    result, at, outs = (summed_on_arrival(both, axis, dim), 0, [])
    for a, column in zip(arrays, columns):
        piece = result[..., at : at + column.shape[along]]
        outs.append(piece.reshape(*piece.shape[:along], *a.shape[along:]))
        at += column.shape[along]
    return tuple(outs)


def joined_along(blocks, dim):
    dims = list(blocks.shape[1:])
    dims[dim] *= blocks.shape[0]
    return jnp.moveaxis(blocks, 0, dim).reshape(dims)


def from_everyone(value, axis):
    copies = jnp.broadcast_to(value, (lax.axis_size(axis), *value.shape))
    return lax.all_to_all(copies, axis, split_axis=0, concat_axis=0, tiled=True)


def collect(value, axis, dim):
    return joined_along(from_everyone(value, axis), dim)


def activate(summed, square_sums, hidden_cols):
    rowscale = lax.rsqrt(square_sums / D + epsilon)[:, None]
    gate_act = summed[:, :hidden_cols] * rowscale
    up_act = summed[:, hidden_cols:] * rowscale
    return (jax.nn.silu(gate_act) * up_act).astype(jnp.bfloat16)


def feed_forward(residual, norm_gain, gate_weight, up_weight, down_weight, finish):
    as_float = residual.astype(jnp.float32)
    squares = jnp.sum(as_float * as_float, axis=1)
    scaled = (as_float * norm_gain).astype(jnp.bfloat16)
    joined = jnp.concatenate([gate_weight, up_weight], axis=1)
    partial_value = jnp.dot(scaled, joined, preferred_element_type=jnp.float32)
    hidden_cols = gate_weight.shape[1]
    summed, square_sums = side_by_side(
        (partial_value.astype(jnp.bfloat16), squares.astype(jnp.bfloat16)), "kv", 0, 1
    )
    hidden = activate(summed, square_sums, hidden_cols)
    projected = jnp.dot(
        collect(hidden, "kv", 0), down_weight, preferred_element_type=jnp.float32
    ).astype(jnp.bfloat16)
    if finish:
        col_count = residual.shape[1] // lax.axis_size("tp")
        own_cols = lax.dynamic_slice_in_dim(
            as_float, lax.axis_index("tp") * col_count, col_count, 1
        )
        branch = summed_on_arrival(projected, "tp", 1)
        return (own_cols + 0.5 * branch).astype(jnp.bfloat16)
    branch = lax.psum(projected, "tp").astype(jnp.float32)
    return (as_float + 0.5 * branch).astype(jnp.bfloat16)


def unit_heads(projected, head_size):
    activated = jax.nn.silu(projected).reshape(projected.shape[0], -1, head_size)
    return activated * lax.rsqrt(jnp.sum(activated * activated, axis=-1, keepdims=True) + epsilon)


def delta_step(old_state, key_rows, queries, values, beta_gate, decay_gate):
    faded_state = old_state * decay_gate[:, :, None, None]
    predicted = jnp.einsum("rhab,rha->rhb", faded_state, key_rows, precision=lax.Precision.HIGHEST)
    correction = beta_gate[:, :, None] * (values - predicted)
    updated = faded_state + key_rows[:, :, :, None] * correction[:, :, None, :]
    reading = jnp.einsum("rhab,rha->rhb", updated, queries, precision=lax.Precision.HIGHEST)
    return (updated, reading)


def token_mixer(
    residual,
    norm_gain,
    query_weight,
    key_weight,
    value_weight,
    output_gate_weight,
    beta_weight,
    decay_weight,
    decay_rate,
    decay_bias,
    head_gain,
    out_weight,
    old_state,
):
    as_float = residual.astype(jnp.float32)
    squares = jnp.sum(as_float * as_float, axis=1)
    scaled = (as_float * norm_gain).astype(jnp.bfloat16)
    joined = jnp.concatenate([query_weight, key_weight, value_weight, output_gate_weight], axis=1)
    partial_value = jnp.dot(scaled, joined, preferred_element_type=jnp.float32)
    heads_dev = decay_rate.shape[0]
    head_start = lax.axis_index("tp") * heads_dev
    gate_cols = jnp.concatenate(
        [
            lax.dynamic_slice_in_dim(beta_weight, head_start, heads_dev, 1),
            lax.dynamic_slice_in_dim(decay_weight, head_start, heads_dev, 1),
        ],
        axis=1,
    )
    gate_part = jnp.dot(scaled, gate_cols, preferred_element_type=jnp.float32)
    row_count = old_state.shape[0]
    summed, gate_summed, square_sums = side_by_side(
        (
            partial_value.astype(jnp.bfloat16),
            gate_part.astype(jnp.bfloat16),
            squares.astype(jnp.bfloat16),
        ),
        "kv",
        0,
        1,
    )
    rowscale = lax.rsqrt(square_sums / D + epsilon)[:, None]
    summed = summed * rowscale
    gate_summed = gate_summed * rowscale
    head_size = old_state.shape[2]
    key_cols = query_weight.shape[1]
    value_cols = value_weight.shape[1]
    repeat_count = heads_dev // (key_cols // head_size)
    queries = jnp.repeat(
        unit_heads(summed[:, :key_cols], head_size) * head_size ** (-0.5), repeat_count, axis=1
    )
    key_rows = jnp.repeat(
        unit_heads(summed[:, key_cols : 2 * key_cols], head_size), repeat_count, axis=1
    )
    values = jax.nn.silu(summed[:, 2 * key_cols : 2 * key_cols + value_cols]).reshape(
        row_count, heads_dev, head_size
    )
    out_gate = jax.nn.silu(summed[:, 2 * key_cols + value_cols :]).reshape(
        row_count, heads_dev, head_size
    )
    beta_gate = jax.nn.sigmoid(gate_summed[:, :heads_dev])
    decay_gate = jnp.exp(
        -jnp.exp(decay_rate)[None, :]
        * jax.nn.softplus(gate_summed[:, heads_dev:] + decay_bias[None, :])
    )
    new_state, reading = delta_step(old_state, key_rows, queries, values, beta_gate, decay_gate)
    normed = reading * lax.rsqrt(jnp.mean(reading * reading, axis=-1, keepdims=True) + epsilon)
    normed = (
        (normed * head_gain * out_gate)
        .reshape(row_count, heads_dev * head_size)
        .astype(jnp.bfloat16)
    )
    projected = jnp.dot(
        collect(normed, "kv", 0), out_weight, preferred_element_type=jnp.float32
    ).astype(jnp.bfloat16)
    branch = lax.psum(projected, "tp").astype(jnp.float32)
    return ((as_float + branch).astype(jnp.bfloat16), new_state)


def body(
    residual_in,
    delta_state,
    norm_gain_first,
    gate_first,
    up_first,
    down_first,
    norm_gain_mixer,
    query_weight,
    key_weight,
    value_weight,
    output_gate_weight,
    beta_weight,
    decay_weight,
    decay_rate,
    decay_bias,
    head_gain,
    out_weight,
    norm_gain_second,
    gate_second,
    up_second,
    down_second,
):
    columns = lax.all_gather(residual_in, "tp", axis=1, tiled=True)
    after_first = feed_forward(columns, norm_gain_first, gate_first, up_first, down_first, False)
    after_mixer, new_state = token_mixer(
        after_first,
        norm_gain_mixer,
        query_weight,
        key_weight,
        value_weight,
        output_gate_weight,
        beta_weight,
        decay_weight,
        decay_rate,
        decay_bias,
        head_gain,
        out_weight,
        delta_state,
    )
    residual_out = feed_forward(
        after_mixer, norm_gain_second, gate_second, up_second, down_second, True
    )
    return (residual_out, new_state)


def solution(mesh):
    placed = (
        P(None, ("kv", "tp")),
        P("kv", "tp", None, None),
        P("kv"),
        P("kv", "tp"),
        P("kv", "tp"),
        P("tp", "kv"),
        P("kv"),
        P("kv", "tp"),
        P("kv", "tp"),
        P("kv", "tp"),
        P("kv", "tp"),
        P("kv", None),
        P("kv", None),
        P("tp"),
        P("tp"),
        P(),
        P("tp", "kv"),
        P("kv"),
        P("kv", "tp"),
        P("kv", "tp"),
        P("tp", "kv"),
    )
    return jax.shard_map(
        body,
        mesh=mesh,
        in_specs=placed,
        out_specs=(P(None, ("kv", "tp")), P("kv", "tp", None, None)),
        check_vma=False,
    )
```

profile of v0, /device:TPU:1, one launch (start us, length us, event | category | flops | bytes accessed | tf_op | source)
XLA Modules:
  0.0 230.6 jit_solution(4892839816095156955)
XLA Ops:
  0.6 16.2 %all_gather.3 = bf16[256,64]{0,1:T(8,128)(2,1)S(1)} all-gather(bf16[256,8]{0,1:T(8,128)(2,1)} %param.21), channel_id=1, replica_groups=mesh['kv'=32,'tp'=8] {'tp'}, dimensions={1}, use_global_device_ids=true | all-gather | bytes 36864 | tf_op jit(solution)/shard_map/all_gather | solution.py:195
  16.9 0.2 convert_element_type.152
  17.1 1.4 fusion
  18.7 31.4 %all_to_all.35 = bf16[32,8,1409]{2,1,0:T(8,128)(2,1)S(1)} all-to-all(bf16[32,8,1409]{2,1,0:T(8,128)(2,1)S(1)} %pad_maximum_fusion), channel_id=1, replica_groups=mesh['kv'=32,'tp'=8] {'kv'}, dimensions={0} | all-to-all | bytes 1442816 | tf_op jit(solution)/shard_map/all_to_all | solution.py:17
  50.4 0.8 broadcast_in_dim.10
  51.2 5.6 %all-to-all-start.1 = ((bf16[32,8,704]{2,1,0:T(8,128)(2,1)}), bf16[32,8,704]{2,1,0:T(8,128)(2,1)S(1)}, u32[]{:S(2)}, u32[]{:S(2)}) async-start(bf16[32,8,704]{2,1,0:T(8,128)(2,1)} %broadcast_in_dim.10), calls=%async_computation.1 | async-start | bytes 786432 | tf_op jit(solution)/shard_map/all_to_all | solution.py:40
  56.8 0.7 constant_dynamic-slice_fusion
  57.5 12.1 %all-to-all-done.1 = bf16[32,8,704]{2,1,0:T(8,128)(2,1)S(1)} async-done(((bf16[32,8,704]{2,1,0:T(8,128)(2,1)}), bf16[32,8,704]{2,1,0:T(8,128)(2,1)S(1)}, u32[]{:S(2)}, u32[]{:S(2)}) %all-to-all-start.1) | async-done | bytes 360480 | tf_op jit(solution)/shard_map/all_to_all | solution.py:40
  69.6 0.2 convolution_convert_fusion.5
  69.8 23.5 %psum.14 = bf16[256,64]{0,1:T(8,128)(2,1)S(1)} all-reduce(bf16[256,64]{0,1:T(8,128)(2,1)S(1)} %convolution_convert_fusion.5), channel_id=1, replica_groups=mesh['kv'=32,'tp'=8] {'tp'}, use_global_device_ids=true, to_apply=%region_2.3 | all-reduce | flops 16384 | bytes 65536 | tf_op jit(solution)/shard_map/psum | solution.py:75
  93.4 0.2 convolution_convert_fusion.6
  93.7 0.2 convert_element_type.153
  94.0 0.5 fusion.1
  94.5 1.1 concatenate.39
  95.6 4.6 %all-to-all-start.2 = ((bf16[32,8,1545]{2,1,0:T(8,128)(2,1)}), bf16[32,8,1545]{2,1,0:T(8,128)(2,1)S(1)}, u32[]{:S(2)}, u32[]{:S(2)}) async-start(bf16[32,8,1545]{2,1,0:T(8,128)(2,1)} %concatenate.39), calls=%async_computation.2 | async-start | bytes 1703936 | tf_op jit(solution)/shard_map/all_to_all | solution.py:17
  100.3 19.5 %all-to-all-done.2 = bf16[32,8,1545]{2,1,0:T(8,128)(2,1)S(1)} async-done(((bf16[32,8,1545]{2,1,0:T(8,128)(2,1)}), bf16[32,8,1545]{2,1,0:T(8,128)(2,1)S(1)}, u32[]{:S(2)}, u32[]{:S(2)}) %all-to-all-start.2) | async-done | bytes 791072 | tf_op jit(solution)/shard_map/all_to_all | solution.py:17
  119.8 0.2 fusion.54
  120.6 2.0 fusion.3
  122.7 0.7 multiply_add_fusion
  123.6 1.2 copy-done.2
  124.8 1.9 fusion.67
  126.9 17.3 %all_to_all.36 = bf16[32,8,512]{2,1,0:T(8,128)(2,1)S(1)} all-to-all(bf16[32,8,512]{2,1,0:T(8,128)(2,1)S(1)} %broadcast_in_dim.13), channel_id=1, replica_groups=mesh['kv'=32,'tp'=8] {'kv'}, dimensions={0} | all-to-all | bytes 524288 | tf_op jit(solution)/shard_map/all_to_all | solution.py:40
  144.2 0.2 convolution_convert_fusion.3
  144.4 26.0 %psum.15 = bf16[256,64]{0,1:T(8,128)(2,1)S(1)} all-reduce(bf16[256,64]{0,1:T(8,128)(2,1)S(1)} %convolution_convert_fusion.3), channel_id=1, replica_groups=mesh['kv'=32,'tp'=8] {'tp'}, use_global_device_ids=true, to_apply=%region_8.9 | all-reduce | flops 16384 | bytes 65536 | tf_op jit(solution)/shard_map/psum | solution.py:168
  170.4 0.2 convert_element_type.154
  170.7 0.5 fusion.2
  171.2 22.8 %all_to_all.37 = bf16[32,8,1409]{2,1,0:T(8,128)(2,1)S(1)} all-to-all(bf16[32,8,1409]{2,1,0:T(8,128)(2,1)S(1)} %pad_maximum_fusion.1), channel_id=1, replica_groups=mesh['kv'=32,'tp'=8] {'kv'}, dimensions={0} | all-to-all | bytes 1442816 | tf_op jit(solution)/shard_map/all_to_all | solution.py:17
  194.4 18.7 %all_to_all.38 = bf16[32,8,704]{2,1,0:T(8,128)(2,1)S(1)} all-to-all(bf16[32,8,704]{2,1,0:T(8,128)(2,1)S(1)} %broadcast_in_dim.14), channel_id=1, replica_groups=mesh['kv'=32,'tp'=8] {'kv'}, dimensions={0} | all-to-all | bytes 720896 | tf_op jit(solution)/shard_map/all_to_all | solution.py:40
  213.1 0.9 fusion.5
  214.0 11.3 %all-to-all-start.6 = ((bf16[8,256,8]{1,2,0:T(8,128)(2,1)}), bf16[8,256,8]{1,2,0:T(8,128)(2,1)S(1)}, u32[]{:S(2)}, u32[]{:S(2)}) async-start(bf16[8,256,8]{1,2,0:T(8,128)(2,1)} %fusion.5), calls=%async_computation.6 | async-start | bytes 65536 | tf_op jit(solution)/shard_map/all_to_all | solution.py:17
  225.2 4.7 %all-to-all-done.6 = bf16[8,256,8]{1,2,0:T(8,128)(2,1)S(1)} async-done(((bf16[8,256,8]{1,2,0:T(8,128)(2,1)}), bf16[8,256,8]{1,2,0:T(8,128)(2,1)S(1)}, u32[]{:S(2)}, u32[]{:S(2)}) %all-to-all-start.6) | async-done | bytes 32800 | tf_op jit(solution)/shard_map/all_to_all | solution.py:17
  230.0 0.6 add_convert_fusion
  (65 shorter events, 2.1 us)
Async XLA Ops:
  0.6 68.9 %copy-start = (bf16[704,64]{0,1:T(8,128)(2,1)S(1)}, bf16[704,64]{0,1:T(8,128)(2,1)}, u32[]{:S(2)}) copy-start(bf16[704,64]{0,1:T(8,128)(2,1)} %param.26) | copy-start | bytes 270340
  18.6 74.8 %copy-start.11 = (f32[64]{0:T(128)S(1)}, f32[64]{0:T(128)}, u32[]{:S(2)}) copy-start(f32[64]{0:T(128)} %param.27) | copy-start | bytes 772
  18.6 75.4 %copy-start.6 = (bf16[64,512]{1,0:T(8,128)(2,1)S(1)}, bf16[64,512]{1,0:T(8,128)(2,1)}, u32[]{:S(2)}) copy-start(bf16[64,512]{1,0:T(8,128)(2,1)} %param.31) | copy-start | bytes 196612
  18.6 75.4 %copy-start.7 = (bf16[64,512]{1,0:T(8,128)(2,1)S(1)}, bf16[64,512]{1,0:T(8,128)(2,1)}, u32[]{:S(2)}) copy-start(bf16[64,512]{1,0:T(8,128)(2,1)} %param.30) | copy-start | bytes 196612
  18.6 75.4 %copy-start.9 = (bf16[64,256]{1,0:T(8,128)(2,1)S(1)}, bf16[64,256]{1,0:T(8,128)(2,1)}, u32[]{:S(2)}) copy-start(bf16[64,256]{1,0:T(8,128)(2,1)} %param.29) | copy-start | bytes 98308
  18.7 75.4 %copy-start.10 = (bf16[64,256]{1,0:T(8,128)(2,1)S(1)}, bf16[64,256]{1,0:T(8,128)(2,1)}, u32[]{:S(2)}) copy-start(bf16[64,256]{1,0:T(8,128)(2,1)} %param.28) | copy-start | bytes 98308
  51.2 18.4 %all-to-all-start.1 = ((bf16[32,8,704]{2,1,0:T(8,128)(2,1)}), bf16[32,8,704]{2,1,0:T(8,128)(2,1)S(1)}, u32[]{:S(2)}, u32[]{:S(2)}) async-start(bf16[32,8,704]{2,1,0:T(8,128)(2,1)} %broadcast_in_dim.10), calls=%async_computation.1 | async-start | bytes 786432 | tf_op jit(solution)/shard_map/all_to_all | solution.py:40
  94.0 6.2 %copy-start.15 = (f32[4]{0:T(128)S(1)}, f32[4]{0:T(128)}, u32[]{:S(2)}) copy-start(f32[4]{0:T(128)} %param.34) | copy-start | bytes 52
  94.5 25.8 %copy-start.14 = (f32[4]{0:T(128)S(1)}, f32[4]{0:T(128)}, u32[]{:S(2)}) copy-start(f32[4]{0:T(128)} %param.35) | copy-start | bytes 52
  94.5 26.1 %copy-start.1 = (f32[8,4,128,128]{3,2,1,0:T(8,128)S(1)}, f32[8,4,128,128]{3,2,1,0:T(8,128)}, u32[]{:S(2)}) copy-start(f32[8,4,128,128]{3,2,1,0:T(8,128)} %param.22) | copy-start | bytes 6291460
  95.6 24.1 %all-to-all-start.2 = ((bf16[32,8,1545]{2,1,0:T(8,128)(2,1)}), bf16[32,8,1545]{2,1,0:T(8,128)(2,1)S(1)}, u32[]{:S(2)}, u32[]{:S(2)}) async-start(bf16[32,8,1545]{2,1,0:T(8,128)(2,1)} %concatenate.39), calls=%async_computation.2 | async-start | bytes 1703936 | tf_op jit(solution)/shard_map/all_to_all | solution.py:17
  123.5 1.3 copy-start.2
  123.5 3.3 %copy-start.13 = (f32[128]{0:T(128)S(1)}, f32[128]{0:T(128)}, u32[]{:S(2)}) copy-start(f32[128]{0:T(128)} %param.36) | copy-start | bytes 1540
  123.5 20.7 %copy-start.8 = (bf16[512,64]{0,1:T(8,128)(2,1)S(1)}, bf16[512,64]{0,1:T(8,128)(2,1)}, u32[]{:S(2)}) copy-start(bf16[512,64]{0,1:T(8,128)(2,1)} %param.37) | copy-start | bytes 196612
  123.5 47.1 %copy-start.3 = (bf16[64,704]{1,0:T(8,128)(2,1)S(1)}, bf16[64,704]{1,0:T(8,128)(2,1)}, u32[]{:S(2)}) copy-start(bf16[64,704]{1,0:T(8,128)(2,1)} %param.40) | copy-start | bytes 270340
  123.5 47.1 %copy-start.4 = (bf16[64,704]{1,0:T(8,128)(2,1)S(1)}, bf16[64,704]{1,0:T(8,128)(2,1)}, u32[]{:S(2)}) copy-start(bf16[64,704]{1,0:T(8,128)(2,1)} %param.39) | copy-start | bytes 270340
  123.5 47.1 %copy-start.12 = (f32[64]{0:T(128)S(1)}, f32[64]{0:T(128)}, u32[]{:S(2)}) copy-start(f32[64]{0:T(128)} %param.38) | copy-start | bytes 772
  171.2 41.9 %copy-start.5 = (bf16[704,64]{0,1:T(8,128)(2,1)S(1)}, bf16[704,64]{0,1:T(8,128)(2,1)}, u32[]{:S(2)}) copy-start(bf16[704,64]{0,1:T(8,128)(2,1)} %param.41) | copy-start | bytes 270340
  214.0 16.0 %all-to-all-start.6 = ((bf16[8,256,8]{1,2,0:T(8,128)(2,1)}), bf16[8,256,8]{1,2,0:T(8,128)(2,1)S(1)}, u32[]{:S(2)}, u32[]{:S(2)}) async-start(bf16[8,256,8]{1,2,0:T(8,128)(2,1)} %fusion.5), calls=%async_computation.6 | async-start | bytes 65536 | tf_op jit(solution)/shard_map/all_to_all | solution.py:17
where the time goes:
time: 231 us
  blocking collectives  156 us (68%)
  waiting for transfers between devices  36.3 us (16%)
  starting transfers between devices  21.5 us (9%)
  matrix products  7.71 us (3%)
  local copies, waits for them, and re-layouts  4.91 us (2%)
  other arithmetic  3.23 us (1%)
    all_to_all x2, blocking collectives, summed_on_arrival(): lax.all_to_all(blocks, axis, split_axis=0, concat_axis=0, tiled=True)  54.2 us
    all_to_all x2, blocking collectives, from_everyone(): return lax.all_to_all(copies, axis, split_axis=0, concat_axis=0, tiled=True)  36 us
    psum x1, blocking collectives, token_mixer(): branch = lax.psum(projected, 'tp').astype(jnp.float32)  26 us
    all_to_all x2, waiting for transfers between devices, summed_on_arrival(): lax.all_to_all(blocks, axis, split_axis=0, concat_axis=0, tiled=True)  24.2 us
    psum x1, blocking collectives, feed_forward(): branch = lax.psum(projected, 'tp').astype(jnp.float32)  23.5 us
    all_gather x1, blocking collectives, body(): columns = lax.all_gather(residual_in, 'tp', axis=1, tiled=True)  16.2 us
    all_to_all x2, starting transfers between devices, summed_on_arrival(): lax.all_to_all(blocks, axis, split_axis=0, concat_axis=0, tiled=True)  15.9 us
    all_to_all x1, waiting for transfers between devices, from_everyone(): return lax.all_to_all(copies, axis, split_axis=0, concat_axis=0, tiled=True)  12.1 us
  transfers between devices with their start and end apart: 3, of which 3 were waited for; matrix products, arithmetic and copies ran while one was open for 0% of the time, Pallas kernels for 0%

commit v1 on v0

--- a/solution.py
+++ b/solution.py
@@ -72,7 +72,7 @@
         )
         branch = summed_on_arrival(projected, "tp", 1)
         return (own_cols + 0.5 * branch).astype(jnp.bfloat16)
-    branch = lax.psum(projected, "tp").astype(jnp.float32)
+    branch = lax.all_gather(projected, "tp").sum(axis=0).astype(jnp.float32)
     return (as_float + 0.5 * branch).astype(jnp.bfloat16)
 
 

time: 231 us -> 221 us (0.957)
  blocking collectives: 156 us -> 143 us
  waiting for transfers between devices: 36.3 us -> 39.6 us
    psum x1 -> x0, blocking collectives: 23.5 us -> none  [feed_forward(): branch = lax.psum(projected, 'tp').astype(jnp.float32)]
    all_gather x0 -> x1, blocking collectives: none -> 16.2 us  [feed_forward(): branch = lax.all_gather(projected, 'tp').sum(axis=0).astype(jnp.float32)]
    all_to_all x2, waiting for transfers between devices: 24.2 us -> 27.5 us  [summed_on_arrival(): lax.all_to_all(blocks, axis, split_axis=0, concat_axis=0, tiled=True)]
where the time goes in v1:
time: 221 us
  blocking collectives  143 us (65%)
  waiting for transfers between devices  39.6 us (18%)
  starting transfers between devices  20.9 us (9%)
  matrix products  7.7 us (3%)
  local copies, waits for them, and re-layouts  4.95 us (2%)
  other arithmetic  3.42 us (2%)
    all_to_all x2, blocking collectives, summed_on_arrival(): lax.all_to_all(blocks, axis, split_axis=0, concat_axis=0, tiled=True)  52.4 us
    all_to_all x2, blocking collectives, from_everyone(): return lax.all_to_all(copies, axis, split_axis=0, concat_axis=0, tiled=True)  34.7 us
    all_to_all x2, waiting for transfers between devices, summed_on_arrival(): lax.all_to_all(blocks, axis, split_axis=0, concat_axis=0, tiled=True)  27.5 us
    psum x1, blocking collectives, token_mixer(): branch = lax.psum(projected, 'tp').astype(jnp.float32)  23.8 us
    all_gather x1, blocking collectives, body(): columns = lax.all_gather(residual_in, 'tp', axis=1, tiled=True)  16.2 us
    all_gather x1, blocking collectives, feed_forward(): branch = lax.all_gather(projected, 'tp').sum(axis=0).astype(jnp.float32)  16.2 us
    all_to_all x2, starting transfers between devices, summed_on_arrival(): lax.all_to_all(blocks, axis, split_axis=0, concat_axis=0, tiled=True)  15.3 us
    all_to_all x1, waiting for transfers between devices, from_everyone(): return lax.all_to_all(copies, axis, split_axis=0, concat_axis=0, tiled=True)  12.1 us
  transfers between devices with their start and end apart: 3, of which 3 were waited for; matrix products, arithmetic and copies ran while one was open for 0% of the time, Pallas kernels for 0%

profile of v1, /device:TPU:1, one launch (start us, length us, event | category | flops | bytes accessed | tf_op | source)
XLA Modules:
  0.0 220.8 jit_solution(6464711819197439719)
XLA Ops:
  0.6 16.2 %all_gather.9 = bf16[256,64]{0,1:T(8,128)(2,1)S(1)} all-gather(bf16[256,8]{0,1:T(8,128)(2,1)} %param.21), channel_id=1, replica_groups=mesh['kv'=32,'tp'=8] {'tp'}, dimensions={1}, use_global_device_ids=true | all-gather | bytes 36864 | tf_op jit(solution)/shard_map/all_gather | solution.py:195
  16.9 0.2 convert_element_type.154
  17.1 1.4 fusion
  18.6 31.3 %all_to_all.35 = bf16[32,8,1409]{2,1,0:T(8,128)(2,1)S(1)} all-to-all(bf16[32,8,1409]{2,1,0:T(8,128)(2,1)S(1)} %pad_maximum_fusion), channel_id=1, replica_groups=mesh['kv'=32,'tp'=8] {'kv'}, dimensions={0} | all-to-all | bytes 1442816 | tf_op jit(solution)/shard_map/all_to_all | solution.py:17
  50.2 0.8 broadcast_in_dim.10
  51.0 5.6 %all-to-all-start.1 = ((bf16[32,8,704]{2,1,0:T(8,128)(2,1)}), bf16[32,8,704]{2,1,0:T(8,128)(2,1)S(1)}, u32[]{:S(2)}, u32[]{:S(2)}) async-start(bf16[32,8,704]{2,1,0:T(8,128)(2,1)} %broadcast_in_dim.10), calls=%async_computation.1 | async-start | bytes 786432 | tf_op jit(solution)/shard_map/all_to_all | solution.py:40
  56.6 0.7 constant_dynamic-slice_fusion
  57.3 12.1 %all-to-all-done.1 = bf16[32,8,704]{2,1,0:T(8,128)(2,1)S(1)} async-done(((bf16[32,8,704]{2,1,0:T(8,128)(2,1)}), bf16[32,8,704]{2,1,0:T(8,128)(2,1)S(1)}, u32[]{:S(2)}, u32[]{:S(2)}) %all-to-all-start.1) | async-done | bytes 360480 | tf_op jit(solution)/shard_map/all_to_all | solution.py:40
  69.4 0.2 convolution_convert_fusion.5
  69.7 16.2 %all-gather = bf16[2048,64]{0,1:T(8,128)(2,1)S(1)} all-gather(bf16[256,64]{0,1:T(8,128)(2,1)S(1)} %convolution_convert_fusion.5), channel_id=2, replica_groups=mesh['kv'=32,'tp'=8] {'tp'}, dimensions={0}, use_global_device_ids=true | all-gather | bytes 294912 | tf_op jit(solution)/shard_map/all_gather | solution.py:75
  85.9 0.2 bitcast_reduce_fusion
  86.1 0.2 convolution_convert_fusion.6
  86.4 0.2 convert_element_type.155
  86.7 0.4 fusion.1
  87.2 1.1 concatenate.39
  88.3 4.0 %all-to-all-start.2 = ((bf16[32,8,1545]{2,1,0:T(8,128)(2,1)}), bf16[32,8,1545]{2,1,0:T(8,128)(2,1)S(1)}, u32[]{:S(2)}, u32[]{:S(2)}) async-start(bf16[32,8,1545]{2,1,0:T(8,128)(2,1)} %concatenate.39), calls=%async_computation.2 | async-start | bytes 1703936 | tf_op jit(solution)/shard_map/all_to_all | solution.py:17
  92.3 22.8 %all-to-all-done.2 = bf16[32,8,1545]{2,1,0:T(8,128)(2,1)S(1)} async-done(((bf16[32,8,1545]{2,1,0:T(8,128)(2,1)}), bf16[32,8,1545]{2,1,0:T(8,128)(2,1)S(1)}, u32[]{:S(2)}, u32[]{:S(2)}) %all-to-all-start.2) | async-done | bytes 791072 | tf_op jit(solution)/shard_map/all_to_all | solution.py:17
  116.0 2.0 fusion.3
  118.1 0.7 multiply_add_fusion
  119.0 1.2 copy-done.2
  120.2 1.9 fusion.67
  122.3 15.9 %all_to_all.36 = bf16[32,8,512]{2,1,0:T(8,128)(2,1)S(1)} all-to-all(bf16[32,8,512]{2,1,0:T(8,128)(2,1)S(1)} %broadcast_in_dim.13), channel_id=1, replica_groups=mesh['kv'=32,'tp'=8] {'kv'}, dimensions={0} | all-to-all | bytes 524288 | tf_op jit(solution)/shard_map/all_to_all | solution.py:40
  138.2 0.2 convolution_convert_fusion.3
  138.4 23.8 %psum.7 = bf16[256,64]{0,1:T(8,128)(2,1)S(1)} all-reduce(bf16[256,64]{0,1:T(8,128)(2,1)S(1)} %convolution_convert_fusion.3), channel_id=1, replica_groups=mesh['kv'=32,'tp'=8] {'tp'}, use_global_device_ids=true, to_apply=%region_8.9 | all-reduce | flops 16384 | bytes 65536 | tf_op jit(solution)/shard_map/psum | solution.py:168
  162.3 0.2 convert_element_type.156
  162.6 0.5 fusion.2
  163.1 21.1 %all_to_all.37 = bf16[32,8,1409]{2,1,0:T(8,128)(2,1)S(1)} all-to-all(bf16[32,8,1409]{2,1,0:T(8,128)(2,1)S(1)} %pad_maximum_fusion.1), channel_id=1, replica_groups=mesh['kv'=32,'tp'=8] {'kv'}, dimensions={0} | all-to-all | bytes 1442816 | tf_op jit(solution)/shard_map/all_to_all | solution.py:17
  184.6 18.7 %all_to_all.38 = bf16[32,8,704]{2,1,0:T(8,128)(2,1)S(1)} all-to-all(bf16[32,8,704]{2,1,0:T(8,128)(2,1)S(1)} %broadcast_in_dim.14), channel_id=1, replica_groups=mesh['kv'=32,'tp'=8] {'kv'}, dimensions={0} | all-to-all | bytes 720896 | tf_op jit(solution)/shard_map/all_to_all | solution.py:40
  203.3 0.9 fusion.5
  204.2 11.3 %all-to-all-start.6 = ((bf16[8,256,8]{1,2,0:T(8,128)(2,1)}), bf16[8,256,8]{1,2,0:T(8,128)(2,1)S(1)}, u32[]{:S(2)}, u32[]{:S(2)}) async-start(bf16[8,256,8]{1,2,0:T(8,128)(2,1)} %fusion.5), calls=%async_computation.6 | async-start | bytes 65536 | tf_op jit(solution)/shard_map/all_to_all | solution.py:17
  215.5 4.7 %all-to-all-done.6 = bf16[8,256,8]{1,2,0:T(8,128)(2,1)S(1)} async-done(((bf16[8,256,8]{1,2,0:T(8,128)(2,1)}), bf16[8,256,8]{1,2,0:T(8,128)(2,1)S(1)}, u32[]{:S(2)}, u32[]{:S(2)}) %all-to-all-start.6) | async-done | bytes 32800 | tf_op jit(solution)/shard_map/all_to_all | solution.py:17
  220.2 0.6 add_convert_fusion
  (67 shorter events, 2.3 us)
Async XLA Ops:
  0.6 68.8 %copy-start = (bf16[704,64]{0,1:T(8,128)(2,1)S(1)}, bf16[704,64]{0,1:T(8,128)(2,1)}, u32[]{:S(2)}) copy-start(bf16[704,64]{0,1:T(8,128)(2,1)} %param.26) | copy-start | bytes 270340
  49.9 36.2 %copy-start.11 = (f32[64]{0:T(128)S(1)}, f32[64]{0:T(128)}, u32[]{:S(2)}) copy-start(f32[64]{0:T(128)} %param.27) | copy-start | bytes 772
  49.9 36.8 %copy-start.6 = (bf16[64,512]{1,0:T(8,128)(2,1)S(1)}, bf16[64,512]{1,0:T(8,128)(2,1)}, u32[]{:S(2)}) copy-start(bf16[64,512]{1,0:T(8,128)(2,1)} %param.31) | copy-start | bytes 196612
  49.9 36.8 %copy-start.7 = (bf16[64,512]{1,0:T(8,128)(2,1)S(1)}, bf16[64,512]{1,0:T(8,128)(2,1)}, u32[]{:S(2)}) copy-start(bf16[64,512]{1,0:T(8,128)(2,1)} %param.30) | copy-start | bytes 196612
  49.9 36.8 %copy-start.9 = (bf16[64,256]{1,0:T(8,128)(2,1)S(1)}, bf16[64,256]{1,0:T(8,128)(2,1)}, u32[]{:S(2)}) copy-start(bf16[64,256]{1,0:T(8,128)(2,1)} %param.29) | copy-start | bytes 98308
  49.9 36.8 %copy-start.10 = (bf16[64,256]{1,0:T(8,128)(2,1)S(1)}, bf16[64,256]{1,0:T(8,128)(2,1)}, u32[]{:S(2)}) copy-start(bf16[64,256]{1,0:T(8,128)(2,1)} %param.28) | copy-start | bytes 98308
  51.0 18.4 %all-to-all-start.1 = ((bf16[32,8,704]{2,1,0:T(8,128)(2,1)}), bf16[32,8,704]{2,1,0:T(8,128)(2,1)S(1)}, u32[]{:S(2)}, u32[]{:S(2)}) async-start(bf16[32,8,704]{2,1,0:T(8,128)(2,1)} %broadcast_in_dim.10), calls=%async_computation.1 | async-start | bytes 786432 | tf_op jit(solution)/shard_map/all_to_all | solution.py:40
  86.7 5.6 %copy-start.15 = (f32[4]{0:T(128)S(1)}, f32[4]{0:T(128)}, u32[]{:S(2)}) copy-start(f32[4]{0:T(128)} %param.34) | copy-start | bytes 52
  87.2 28.5 %copy-start.14 = (f32[4]{0:T(128)S(1)}, f32[4]{0:T(128)}, u32[]{:S(2)}) copy-start(f32[4]{0:T(128)} %param.35) | copy-start | bytes 52
  87.2 28.8 %copy-start.1 = (f32[8,4,128,128]{3,2,1,0:T(8,128)S(1)}, f32[8,4,128,128]{3,2,1,0:T(8,128)}, u32[]{:S(2)}) copy-start(f32[8,4,128,128]{3,2,1,0:T(8,128)} %param.22) | copy-start | bytes 6291460
  88.3 26.8 %all-to-all-start.2 = ((bf16[32,8,1545]{2,1,0:T(8,128)(2,1)}), bf16[32,8,1545]{2,1,0:T(8,128)(2,1)S(1)}, u32[]{:S(2)}, u32[]{:S(2)}) async-start(bf16[32,8,1545]{2,1,0:T(8,128)(2,1)} %concatenate.39), calls=%async_computation.2 | async-start | bytes 1703936 | tf_op jit(solution)/shard_map/all_to_all | solution.py:17
  118.9 1.3 copy-start.2
  118.9 3.3 %copy-start.13 = (f32[128]{0:T(128)S(1)}, f32[128]{0:T(128)}, u32[]{:S(2)}) copy-start(f32[128]{0:T(128)} %param.36) | copy-start | bytes 1540
  118.9 19.3 %copy-start.8 = (bf16[512,64]{0,1:T(8,128)(2,1)S(1)}, bf16[512,64]{0,1:T(8,128)(2,1)}, u32[]{:S(2)}) copy-start(bf16[512,64]{0,1:T(8,128)(2,1)} %param.37) | copy-start | bytes 196612
  118.9 43.6 %copy-start.3 = (bf16[64,704]{1,0:T(8,128)(2,1)S(1)}, bf16[64,704]{1,0:T(8,128)(2,1)}, u32[]{:S(2)}) copy-start(bf16[64,704]{1,0:T(8,128)(2,1)} %param.40) | copy-start | bytes 270340
  118.9 43.6 %copy-start.4 = (bf16[64,704]{1,0:T(8,128)(2,1)S(1)}, bf16[64,704]{1,0:T(8,128)(2,1)}, u32[]{:S(2)}) copy-start(bf16[64,704]{1,0:T(8,128)(2,1)} %param.39) | copy-start | bytes 270340
  118.9 43.6 %copy-start.12 = (f32[64]{0:T(128)S(1)}, f32[64]{0:T(128)}, u32[]{:S(2)}) copy-start(f32[64]{0:T(128)} %param.38) | copy-start | bytes 772
  163.1 40.2 %copy-start.5 = (bf16[704,64]{0,1:T(8,128)(2,1)S(1)}, bf16[704,64]{0,1:T(8,128)(2,1)}, u32[]{:S(2)}) copy-start(bf16[704,64]{0,1:T(8,128)(2,1)} %param.41) | copy-start | bytes 270340
  204.2 16.0 %all-to-all-start.6 = ((bf16[8,256,8]{1,2,0:T(8,128)(2,1)}), bf16[8,256,8]{1,2,0:T(8,128)(2,1)S(1)}, u32[]{:S(2)}, u32[]{:S(2)}) async-start(bf16[8,256,8]{1,2,0:T(8,128)(2,1)} %fusion.5), calls=%async_computation.6 | async-start | bytes 65536 | tf_op jit(solution)/shard_map/all_to_all | solution.py:17
